TPU v7x, 128 devices: a whole 4x4x4 slice. The times are simulated.
128 devices in a mesh: ep: 16 (over z, x), tp: 8 (over y, core).
Axes of the slice: x: 4, y: 4, z: 4, core: 2. Of those that a mesh axis runs over, the one named last changes fastest.
Arguments:
- residual: bfloat16 [2048, 2048], P('ep', 'tp'), may hold values from -61 to 61
- in_gain: float32 [2048], replicated, may hold values from 0.1 to 1.9
- in_weight: bfloat16 [2048, 1024], P(None, 'tp'), may hold values from -0.125 to 0.125
- state: float32 [2, 2048, 4096], P(None, 'ep', 'tp'), may hold values from -3 to 3
- decay_rate: float32 [64, 64], P('tp'), may hold values from 0.1 to 1
- frequency: float32 [64, 64], P('tp'), may hold values from 0 to 200
- log_step: float32 [64], P('tp'), may hold values from -3 to -0.7
- in_coef: float32 [2, 64, 64, 16], P(None, 'tp'), may hold values from -1 to 1
- out_coef: float32 [2, 64, 16, 64], P(None, 'tp'), may hold values from -0.75 to 0.75
- skip_gain: float32 [1024], P('tp'), may hold values from -3 to 3
- out_weight: bfloat16 [1024, 2048], replicated, may hold values from -0.1875 to 0.1875
- mid_gain: float32 [2048], replicated, may hold values from 0.1 to 1.9
- gate_vector: bfloat16 [2048], replicated, may hold values from -0.125 to 0.125
- routes: int32 [2048, 4], P('ep'), may hold values from 0 to 127, all different within a row; in each aligned block of 128 rows (0 to 127, 128 to 255, ...) at most 8 rows name the same one
- route_weight: float32 [2048, 4], P('ep'), may hold values from 0.1 to 1
- expert_gate: bfloat16 [128, 2048, 512], P(('ep', 'tp')), may hold values from -0.125 to 0.125
- expert_up: bfloat16 [128, 2048, 512], P(('ep', 'tp')), may hold values from -0.125 to 0.125
- expert_down: bfloat16 [128, 512, 2048], P(('ep', 'tp')), may hold values from -0.25 to 0.25
- shared_gate: bfloat16 [2048, 4096], P(None, 'ep'), may hold values from -0.125 to 0.125
- shared_up: bfloat16 [2048, 4096], P(None, 'ep'), may hold values from -0.125 to 0.125
- shared_down: bfloat16 [4096, 2048], P('ep'), may hold values from -0.09375 to 0.09375
Outputs:
- layer_out: bfloat16 [2048, 2048], P(('ep', 'tp'))
- new_state: float32 [2, 2048, 4096], P(None, 'ep', 'tp')
Inputs may be any that keep to these rules, and one draw needn't show every extreme that they name: `routes`: each row names 4 different experts. Among the rows of one index of ep no expert is named more than 8 times, a bound that some block reaches.
All inputs are finite; a program needn't handle non-finite values.
Results may differ from a plain program's by a relative error of at most 0.0085.
Values may be sent and summed in bfloat16 or wider, within the bound.
No kernel may reach another device: no remote copies, remote signals or barrier semaphores. Data moves between devices by JAX's collectives and lax.ppermute only.
A program may use at most 128 MiB of HBM per device.

v0:
```python
import jax
import jax.numpy as jnp
from jax import lax
from jax.sharding import PartitionSpec as P

norm_eps = 1e-05
routed_scale = 2.5


def laid_out(blocks, dim):
    dims = list(blocks.shape[1:])
    dims[dim] *= blocks.shape[0]
    return jnp.moveaxis(blocks, 0, dim).reshape(dims)


def from_everyone(array, axis):
    length = lax.axis_size(axis)
    return lax.all_to_all(
        jnp.broadcast_to(array[None], (length, *array.shape)), axis, 0, 0, tiled=True
    )


def gather_directly(array, axis, dim):
    return laid_out(from_everyone(array, axis), dim)


def in_one_piece(arrays, axis, split_dim, concat_dim, along):
    both = jnp.concatenate(arrays, axis=along)
    result, at, finished = (
        lax.all_to_all(both, axis, split_axis=split_dim, concat_axis=concat_dim, tiled=True),
        0,
        [],
    )
    for a in arrays:
        finished.append(lax.slice_in_dim(result, at, at + a.shape[along], axis=along))
        at += a.shape[along]
    return tuple(finished)


def in_blocks(array, dim, length):
    before, after = (array.shape[:dim], array.shape[dim + 1 :])
    return jnp.moveaxis(array.reshape(*before, length, -1, *after), dim, 0)


def sent_and_summed(array, axis, dim):
    length = lax.axis_size(axis)
    blocks = lax.all_to_all(in_blocks(array, dim, length), axis, 0, 0, tiled=True)
    return jnp.sum(blocks.astype(jnp.float32), axis=0)


def layer_norm(values, gain_vec):
    row_mean = jnp.mean(values, axis=-1, keepdims=True)
    row_square = jnp.mean(values * values, axis=-1, keepdims=True)
    return (values - row_mean) * lax.rsqrt(row_square - row_mean * row_mean + norm_eps) * gain_vec


def coefficients(decay_rate, frequency, log_step, in_coef):
    time_step = jnp.exp(log_step)[:, None]
    real_rate = -decay_rate
    magnitude = jnp.exp(real_rate * time_step)
    keep_re = magnitude * jnp.cos(frequency * time_step)
    keep_im = magnitude * jnp.sin(frequency * time_step)
    denominator = real_rate * real_rate + frequency * frequency
    factor_re = ((keep_re - 1.0) * real_rate + keep_im * frequency) / denominator
    factor_im = (keep_im * real_rate - (keep_re - 1.0) * frequency) / denominator
    push_re = factor_re[..., None] * in_coef[0] - factor_im[..., None] * in_coef[1]
    push_im = factor_re[..., None] * in_coef[1] + factor_im[..., None] * in_coef[0]
    return (keep_re, keep_im, push_re, push_im)


def mixer_step(
    normed, in_weight, state, decay_rate, frequency, log_step, in_coef, out_coef, skip_gain
):
    row_count = normed.shape[0]
    group_count, state_count = decay_rate.shape
    keep_re, keep_im, push_re, push_im = coefficients(decay_rate, frequency, log_step, in_coef)
    drive = jnp.dot(normed, in_weight, preferred_element_type=jnp.float32).astype(jnp.bfloat16)
    drive_f = drive.astype(jnp.float32).reshape(row_count, group_count, -1)
    input_re = jnp.einsum("tgh,gph->tgp", drive_f, push_re)
    input_im = jnp.einsum("tgh,gph->tgp", drive_f, push_im)
    old_re = state[0].reshape(row_count, group_count, state_count)
    old_im = state[1].reshape(row_count, group_count, state_count)
    new_re = keep_re * old_re - keep_im * old_im + input_re
    new_im = keep_re * old_im + keep_im * old_re + input_im
    read_out = jnp.einsum("ghp,tgp->tgh", out_coef[0], new_re) - jnp.einsum(
        "ghp,tgp->tgh", out_coef[1], new_im
    )
    read_out = read_out.reshape(row_count, -1) + skip_gain * drive_f.reshape(row_count, -1)
    mixed_rows = jax.nn.gelu(read_out, approximate=True).astype(jnp.bfloat16)
    updated = jnp.stack([new_re.reshape(row_count, -1), new_im.reshape(row_count, -1)])
    return (mixed_rows, updated)


def route_slots(routes, experts):
    flat_routes = routes.reshape(-1)
    onehot = (flat_routes[:, None] == jnp.arange(experts, dtype=jnp.int32)[None, :]).astype(
        jnp.int32
    )
    before = jnp.cumsum(onehot, axis=0) - onehot
    return jnp.sum(before * onehot, axis=1).reshape(routes.shape)


def expert_block(row_block, gate_weight, up_weight, down_weight):
    gate_part = jnp.dot(row_block, gate_weight, preferred_element_type=jnp.float32)
    up_part = jnp.dot(row_block, up_weight, preferred_element_type=jnp.float32)
    hidden = (jax.nn.silu(gate_part) * up_part).astype(jnp.bfloat16)
    return jnp.dot(hidden, down_weight, preferred_element_type=jnp.float32).astype(jnp.bfloat16)


def per_device(
    residual,
    in_gain,
    in_weight,
    state,
    decay_rate,
    frequency,
    log_step,
    in_coef,
    out_coef,
    skip_gain,
    out_weight,
    mid_gain,
    gate_vector,
    routes,
    route_weight,
    expert_gate,
    expert_up,
    expert_down,
    shared_gate,
    shared_up,
    shared_down,
):
    tp_count = lax.axis_size("tp")
    ep_count = lax.axis_size("ep")
    tp_place = lax.axis_index("tp")
    seq_rows, feat_part = residual.shape
    width = feat_part * tp_count
    full_resid = gather_directly(residual, "tp", 1)
    normed = layer_norm(full_resid.astype(jnp.float32), in_gain).astype(jnp.bfloat16)
    mixed_part, new_state = mixer_step(
        normed, in_weight, state, decay_rate, frequency, log_step, in_coef, out_coef, skip_gain
    )
    mixed_rows = lax.all_gather(mixed_part, "tp", axis=1, tiled=True)
    after_mix = full_resid.astype(jnp.float32) + jnp.dot(
        mixed_rows, out_weight, preferred_element_type=jnp.float32
    )
    normed_mid = layer_norm(after_mix, mid_gain).astype(jnp.bfloat16)
    per_dev = seq_rows // tp_count
    own_mid = lax.dynamic_slice_in_dim(normed_mid, tp_place * per_dev, per_dev, 0)
    own_after = lax.dynamic_slice_in_dim(after_mix, tp_place * per_dev, per_dev, 0)
    experts = ep_count * tp_count
    top_count = routes.shape[1]
    capacity = max(2, 2 * seq_rows * top_count // experts)
    slot_rank = route_slots(routes, experts)
    dest_tp = routes % tp_count
    dest_ep = routes // tp_count
    is_mine = dest_tp == tp_place
    slot_place = dest_ep * capacity + slot_rank
    slot_total = ep_count * capacity
    matches = (
        slot_place.reshape(-1)[None, :] == jnp.arange(slot_total, dtype=jnp.int32)[:, None]
    ) & is_mine.reshape(-1)[None, :]
    token_ids = jnp.repeat(jnp.arange(seq_rows, dtype=jnp.int32), top_count)
    slot_token = jnp.sum(jnp.where(matches, token_ids[None, :], 0), axis=1)
    outgoing = normed_mid[slot_token].reshape(ep_count, capacity, width)
    copies = jnp.broadcast_to(own_mid[None], (ep_count, per_dev, width))
    got_slots, got_rows = in_one_piece((outgoing, copies), "ep", 0, 0, 1)
    flat_rows = got_slots.reshape(-1, width)
    result = expert_block(flat_rows, expert_gate[0], expert_up[0], expert_down[0])
    computed = result.reshape(got_slots.shape)
    returned = lax.all_to_all(computed, "ep", split_axis=0, concat_axis=0, tiled=True)
    piece = got_rows.reshape(-1, width)
    gate_part = jnp.dot(piece, shared_gate, preferred_element_type=jnp.float32)
    up_part = jnp.dot(piece, shared_up, preferred_element_type=jnp.float32)
    shared_hidden = (jax.nn.silu(gate_part) * up_part).astype(jnp.bfloat16)
    partial_rows = jnp.dot(shared_hidden, shared_down, preferred_element_type=jnp.float32)
    partial_back = lax.all_to_all(
        partial_rows.reshape(ep_count, per_dev, width).astype(jnp.bfloat16),
        "ep",
        split_axis=0,
        concat_axis=0,
        tiled=True,
    ).astype(jnp.float32)
    shared = jnp.sum(partial_back, axis=0)
    flat_back = returned.reshape(slot_total, width)
    weights = route_weight / jnp.sum(route_weight, axis=-1, keepdims=True) * routed_scale
    picked = flat_back[jnp.where(is_mine, slot_place, 0)].astype(jnp.float32)
    routed_part = jnp.sum(jnp.where(is_mine, weights, 0.0)[..., None] * picked, axis=1)
    routed = sent_and_summed(routed_part.astype(jnp.bfloat16), "tp", 0)
    gate_value = jax.nn.sigmoid(jnp.dot(own_mid, gate_vector, preferred_element_type=jnp.float32))
    layer_out = (own_after + routed + gate_value[:, None] * shared).astype(jnp.bfloat16)
    return (layer_out, new_state)


def solution(mesh):
    return jax.shard_map(
        per_device,
        mesh=mesh,
        in_specs=(
            P("ep", "tp"),
            P(),
            P(None, "tp"),
            P(None, "ep", "tp"),
            P("tp", None),
            P("tp", None),
            P("tp"),
            P(None, "tp", None, None),
            P(None, "tp", None, None),
            P("tp"),
            P(),
            P(),
            P(),
            P("ep", None),
            P("ep", None),
            P(("ep", "tp"), None, None),
            P(("ep", "tp"), None, None),
            P(("ep", "tp"), None, None),
            P(None, "ep"),
            P(None, "ep"),
            P("ep", None),
        ),
        out_specs=(P(("ep", "tp"), None), P(None, "ep", "tp")),
        check_vma=False,
    )
```

profile of v0, /device:TPU:0, one launch (start us, length us, event | category | flops | bytes accessed | tf_op | source)
XLA Modules:
  0.0 138.5 jit_solution(16512454888797237247)
XLA Ops:
  0.7 1.8 %broadcast_in_dim.22 = bf16[8,128,256]{2,1,0:T(8,128)(2,1)} broadcast(bf16[128,256]{1,0:T(8,128)(2,1)} %param.21), dimensions={1,2} | broadcast | bytes 589824 | tf_op jit(solution)/shard_map/broadcast_in_dim | solution.py:19
  2.5 4.6 %all-to-all-start = ((bf16[8,128,256]{2,1,0:T(8,128)(2,1)}), bf16[8,128,256]{2,1,0:T(8,128)(2,1)S(1)}, u32[]{:S(2)}, u32[]{:S(2)}) async-start(bf16[8,128,256]{2,1,0:T(8,128)(2,1)} %broadcast_in_dim.22), calls=%async_computation | async-start | bytes 1048576 | tf_op jit(solution)/shard_map/all_to_all | solution.py:18
  7.1 0.8 copy.88
  7.8 0.1 eq.54
  8.0 0.1 eq.50
  8.1 0.7 exp.17
  8.7 0.7 reduce_sum.94
  9.4 0.7 multiply_select_fusion
  10.1 0.1 copy.94
  10.3 0.1 and.23
  10.4 0.1 copy.90
  10.6 0.1 broadcast_in_dim.25
  10.7 0.2 fusion.37
  11.0 0.2 fusion.26
  11.2 0.1 reshape.121
  11.4 0.1 copy.93
  11.5 0.1 eq.58
  11.6 1.1 fusion.78
  12.7 0.1 copy.85
  12.8 0.1 copy.86
  13.0 0.1 select_reduce_fusion
  13.2 0.1 add_divide_fusion
  13.3 4.1 %all-to-all-done = bf16[8,128,256]{2,1,0:T(8,128)(2,1)S(1)} async-done(((bf16[8,128,256]{2,1,0:T(8,128)(2,1)}), bf16[8,128,256]{2,1,0:T(8,128)(2,1)S(1)}, u32[]{:S(2)}, u32[]{:S(2)}) %all-to-all-start) | async-done | bytes 524320 | tf_op jit(solution)/shard_map/all_to_all | solution.py:18
  17.6 0.2 convert_reduce_fusion.1
  17.8 0.6 copy-done.7
  18.4 0.4 convolution_convert_fusion.2
  18.9 0.3 fusion.9
  19.2 0.3 fusion.10
  19.5 0.1 fusion.52
  19.6 0.1 convolution_subtract_fusion
  19.8 0.1 fusion.50
  19.9 12.8 %all_gather.3 = bf16[128,1024]{0,1:T(8,128)(2,1)S(1)} all-gather(bf16[128,128]{0,1:T(8,128)(2,1)S(1)} %fusion.50), channel_id=1, replica_groups=mesh['ep'=16,'tp'=8] {'tp'}, dimensions={1}, use_global_device_ids=true | all-gather | bytes 294912 | tf_op jit(solution)/shard_map/all_gather | solution.py:143
  32.7 0.8 fusion.75
  33.6 1.0 copy-done.2
  34.6 0.2 multiply_convert_fusion
  34.8 0.9 gather_fusion
  35.8 0.1 broadcast_in_dim.32
  35.9 0.2 pad_maximum_fusion
  36.1 31.1 %all_to_all.25 = bf16[16,24,2048]{2,1,0:T(8,128)(2,1)S(1)} all-to-all(bf16[16,24,2048]{2,1,0:T(8,128)(2,1)S(1)} %pad_maximum_fusion), channel_id=1, replica_groups=mesh['ep'=16,'tp'=8] {'ep'}, dimensions={0} | all-to-all | bytes 3145728 | tf_op jit(solution)/shard_map/all_to_all | solution.py:30
  67.1 1.2 copy-done.1
  68.3 0.4 fusion.4
  68.8 3.4 %fusion = bf16[16,8,2048]{2,1,0:T(8,128)(2,1)} fusion(bf16[1,512,2048]{2,1,0:T(8,128)(2,1)S(1)} %copy-done, bf16[1,2048,512]{2,1,0:T(8,128)(2,1)} %param.37, bf16[16,24,2048]{2,1,0:T(8,128)(2,1)} %copy-done.1, f32[128,512]{1,0:T(8,128)S(1)} %fusion.4), kind=kOutput, calls=%fused_computation.6 | convolution fusion | flops 537526272 | bytes 5505024 | tf_op jit(solution)/shard_map/dot_general | solution.py:107
  72.2 3.6 %all-to-all-start.2 = ((bf16[16,8,2048]{2,1,0:T(8,128)(2,1)}), bf16[16,8,2048]{2,1,0:T(8,128)(2,1)S(1)}, u32[]{:S(2)}, u32[]{:S(2)}) async-start(bf16[16,8,2048]{2,1,0:T(8,128)(2,1)} %fusion), calls=%async_computation.2 | async-start | bytes 1048576 | tf_op jit(solution)/shard_map/all_to_all | solution.py:171
  75.7 0.1 copy.87
  75.9 0.1 copy.95
  76.0 0.1 reshape.138
  76.1 2.3 %slice.48 = bf16[16,16,2048]{2,1,0:T(8,128)(2,1)} slice(bf16[16,24,2048]{2,1,0:T(8,128)(2,1)} %copy-done.1), slice={[0:16], [8:24], [0:2048]} | slice | bytes 2097152 | tf_op jit(solution)/shard_map/slice | solution.py:35
  78.4 8.2 %all-to-all-done.2 = bf16[16,8,2048]{2,1,0:T(8,128)(2,1)S(1)} async-done(((bf16[16,8,2048]{2,1,0:T(8,128)(2,1)}), bf16[16,8,2048]{2,1,0:T(8,128)(2,1)S(1)}, u32[]{:S(2)}, u32[]{:S(2)}) %all-to-all-start.2) | async-done | bytes 524320 | tf_op jit(solution)/shard_map/all_to_all | solution.py:171
  86.6 3.3 %gather_fusion.1 = bf16[512,2048]{1,0:T(8,128)(2,1)} fusion(bf16[128,2048]{1,0:T(8,128)(2,1)S(1)} %bitcast.115, s32[1024]{0:T(1024)S(1)} %pad_clamp_fusion), kind=kCustom, calls=%fused_computation.1 | custom fusion | bytes 4196352 | tf_op jit(solution)/shard_map/gather | solution.py:187
  89.9 4.8 %reshape.146 = f32[128,4,2048]{2,1,0:T(4,128)} reshape(bf16[512,2048]{1,0:T(8,128)(2,1)} %gather_fusion.1) | data formatting | bytes 6291456 | tf_op jit(solution)/shard_map/convert_element_type | solution.py:187
  94.7 6.3 %multiply_reduce_fusion = bf16[128,2048]{1,0:T(8,128)(2,1)} fusion(f32[128,4,2048]{2,1,0:T(4,128)} %reshape.146, f32[128,4]{1,0:T(8,128)S(1)} %copy.87), kind=kLoop, calls=%fused_computation.2 | loop fusion | flops 1835008 | bytes 4720640 | tf_op jit(solution)/shard_map/reduce_sum | solution.py:188
  100.9 4.1 %all-to-all-start.3 = ((bf16[8,16,2048]{2,1,0:T(8,128)(2,1)}), bf16[8,16,2048]{2,1,0:T(8,128)(2,1)}, u32[]{:S(2)}, u32[]{:S(2)}) async-start(bf16[8,16,2048]{2,1,0:T(8,128)(2,1)} %bitcast.126), calls=%async_computation.3 | async-start | bytes 1048576 | tf_op jit(solution)/shard_map/all_to_all | solution.py:47
  105.1 2.4 %fusion.79 = f32[256,256]{1,0:T(8,128)} fusion(bf16[256,2048]{1,0:T(8,128)(2,1)S(1)} %bitcast.118, bf16[2048,256]{1,0:T(8,128)(2,1)} %param.39), kind=kOutput, calls=%fused_computation.129 | convolution fusion | flops 268435456 | bytes 2359296 | tf_op jit(solution)/shard_map/dot_general | solution.py:173
  107.5 3.9 %convolution_convert_fusion = bf16[256,2048]{1,0:T(8,128)(2,1)} fusion(bf16[256,2048]{1,0:T(8,128)(2,1)} %param.41, bf16[256,2048]{1,0:T(8,128)(2,1)S(1)} %bitcast.119, bf16[2048,256]{1,0:T(8,128)(2,1)} %param.40, f32[256,256]{1,0:T(8,128)} %fusion.79), kind=kOutput, calls=%fused_computation.3 | convolution fusion | flops 537788416 | bytes 4456448 | tf_op jit(solution)/shard_map/dot_general | solution.py:176
  111.4 4.0 %all-to-all-done.3 = bf16[8,16,2048]{2,1,0:T(8,128)(2,1)} async-done(((bf16[8,16,2048]{2,1,0:T(8,128)(2,1)}), bf16[8,16,2048]{2,1,0:T(8,128)(2,1)}, u32[]{:S(2)}, u32[]{:S(2)}) %all-to-all-start.3) | async-done | bytes 524320 | tf_op jit(solution)/shard_map/all_to_all | solution.py:47
  115.4 3.7 %all-to-all-start.4 = ((bf16[16,16,2048]{2,1,0:T(8,128)(2,1)}), bf16[16,16,2048]{2,1,0:T(8,128)(2,1)S(1)}, u32[]{:S(2)}, u32[]{:S(2)}) async-start(bf16[16,16,2048]{2,1,0:T(8,128)(2,1)} %bitcast.129), calls=%async_computation.4 | async-start | bytes 2097152 | tf_op jit(solution)/shard_map/all_to_all | solution.py:177
  119.1 1.8 %copy.97 = f32[1,128,512]{2,1,0:T(8,128)} copy(f32[1,128,512]{1,2,0:T(8,128)} %bitcast.125) | data formatting | bytes 524288 | tf_op jit(solution)/shard_map/stack;reshape | solution.py:90
  120.9 0.8 copy.96
  121.7 1.9 %pad_maximum_fusion.1 = f32[2,128,512]{2,1,0:T(8,128)} fusion(f32[1,128,512]{2,1,0:T(8,128)} %copy.97, f32[1,128,512]{2,1,0:T(8,128)} %copy.96), kind=kLoop, calls=%fused_computation.38 | loop fusion | flops 131072 | bytes 1048576 | tf_op jit(solution)/shard_map/stack | solution.py:90
  123.6 0.1 fusion.18
  123.7 1.1 convert_reduce_fusion.2
  124.9 11.8 %all-to-all-done.4 = bf16[16,16,2048]{2,1,0:T(8,128)(2,1)S(1)} async-done(((bf16[16,16,2048]{2,1,0:T(8,128)(2,1)}), bf16[16,16,2048]{2,1,0:T(8,128)(2,1)S(1)}, u32[]{:S(2)}, u32[]{:S(2)}) %all-to-all-start.4) | async-done | bytes 1048608 | tf_op jit(solution)/shard_map/all_to_all | solution.py:177
  136.7 0.1 convert_reduce_fusion
  136.8 1.6 %add_convert_fusion = bf16[16,2048]{1,0:T(8,128)(2,1)} fusion(f32[16,2048]{1,0:T(8,128)S(1)} %convert_reduce_fusion, f32[16,2048]{1,0:T(8,128)S(1)} %convert_reduce_fusion.2, f32[128,2048]{1,0:T(8,128)} %copy-done.2, s32[]{:T(128)S(6)} %select_n.41, f32[16]{0:T(128)S(1)} %fusion.18), kind=kLoop, calls=%fused_computation.62 | loop fusion | flops 131072 | bytes 458820 | tf_op jit(solution)/shard_map/convert_element_type | solution.py:191
  (49 shorter events, 0.5 us)
Async XLA Ops:
  0.6 68.1 %copy-start = (bf16[1,512,2048]{2,1,0:T(8,128)(2,1)S(1)}, bf16[1,512,2048]{2,1,0:T(8,128)(2,1)}, u32[]{:S(2)}) copy-start(bf16[1,512,2048]{2,1,0:T(8,128)(2,1)} %param.38) | copy-start | bytes 6291460
  0.6 10.7 %copy-start.10 = (s32[128,4]{0,1:T(4,128)S(1)}, s32[128,4]{0,1:T(4,128)}, u32[]{:S(2)}) copy-start(s32[128,4]{0,1:T(4,128)} %param.34) | copy-start | bytes 6148
  2.5 14.9 %all-to-all-start = ((bf16[8,128,256]{2,1,0:T(8,128)(2,1)}), bf16[8,128,256]{2,1,0:T(8,128)(2,1)S(1)}, u32[]{:S(2)}, u32[]{:S(2)}) async-start(bf16[8,128,256]{2,1,0:T(8,128)(2,1)} %broadcast_in_dim.22), calls=%async_computation | async-start | bytes 1048576 | tf_op jit(solution)/shard_map/all_to_all | solution.py:18
  10.5 2.6 %copy-start.13 = (f32[8,64]{1,0:T(8,128)S(1)}, f32[8,64]{1,0:T(8,128)}, u32[]{:S(2)}) copy-start(f32[8,64]{1,0:T(8,128)} %param.26) | copy-start | bytes 6148
  10.5 2.6 %copy-start.14 = (f32[8,64]{1,0:T(8,128)S(1)}, f32[8,64]{1,0:T(8,128)}, u32[]{:S(2)}) copy-start(f32[8,64]{1,0:T(8,128)} %param.25) | copy-start | bytes 6148
  13.3 4.6 %copy-start.11 = (f32[2048]{0:T(1024)S(1)}, f32[2048]{0:T(1024)}, u32[]{:S(2)}) copy-start(f32[2048]{0:T(1024)} %param.22) | copy-start | bytes 24580
  17.4 1.0 copy-start.7
  17.5 1.4 copy-start.8
  17.6 1.9 %copy-start.9 = (f32[2,8,16,64]{3,2,1,0:T(8,128)S(1)}, f32[2,8,16,64]{3,2,1,0:T(8,128)}, u32[]{:S(2)}) copy-start(f32[2,8,16,64]{3,2,1,0:T(8,128)} %param.29) | copy-start | bytes 196612
  18.4 1.4 copy-start.16
  18.4 14.3 %copy-start.3 = (bf16[1024,2048]{1,0:T(8,128)(2,1)S(1)}, bf16[1024,2048]{1,0:T(8,128)(2,1)}, u32[]{:S(2)}) copy-start(bf16[1024,2048]{1,0:T(8,128)(2,1)} %param.31) | copy-start | bytes 12582916
  19.2 14.4 %copy-start.5 = (f32[128,8,64]{0,2,1:T(8,128)}, f32[128,8,64]{0,2,1:T(8,128)S(1)}, u32[]{:S(2)}) copy-start(f32[128,8,64]{0,2,1:T(8,128)S(1)} %fusion.9) | copy-start | bytes 786436
  32.7 1.9 %copy-start.12 = (f32[2048]{0:T(1024)S(1)}, f32[2048]{0:T(1024)}, u32[]{:S(2)}) copy-start(f32[2048]{0:T(1024)} %param.32) | copy-start | bytes 24580
  33.6 1.0 copy-start.2
  36.0 32.3 %copy-start.6 = (bf16[1,2048,512]{2,1,0:T(8,128)(2,1)S(1)}, bf16[1,2048,512]{2,1,0:T(8,128)(2,1)}, u32[]{:S(2)}) copy-start(bf16[1,2048,512]{2,1,0:T(8,128)(2,1)} %param.36) | copy-start | bytes 6291460
  67.1 1.2 copy-start.1
  72.2 14.4 %all-to-all-start.2 = ((bf16[16,8,2048]{2,1,0:T(8,128)(2,1)}), bf16[16,8,2048]{2,1,0:T(8,128)(2,1)S(1)}, u32[]{:S(2)}, u32[]{:S(2)}) async-start(bf16[16,8,2048]{2,1,0:T(8,128)(2,1)} %fusion), calls=%async_computation.2 | async-start | bytes 1048576 | tf_op jit(solution)/shard_map/all_to_all | solution.py:171
  94.7 10.4 %copy-start.4 = (bf16[16,16,2048]{2,1,0:T(8,128)(2,1)S(1)}, bf16[16,16,2048]{2,1,0:T(8,128)(2,1)}, u32[]{:S(2)}) copy-start(bf16[16,16,2048]{2,1,0:T(8,128)(2,1)} %slice.48) | copy-start | bytes 3145732
  100.9 14.5 %all-to-all-start.3 = ((bf16[8,16,2048]{2,1,0:T(8,128)(2,1)}), bf16[8,16,2048]{2,1,0:T(8,128)(2,1)}, u32[]{:S(2)}, u32[]{:S(2)}) async-start(bf16[8,16,2048]{2,1,0:T(8,128)(2,1)} %bitcast.126), calls=%async_computation.3 | async-start | bytes 1048576 | tf_op jit(solution)/shard_map/all_to_all | solution.py:47
  111.4 7.7 %copy-start.15 = (bf16[2048]{0:T(1024)(128)(2,1)S(1)}, bf16[2048]{0:T(1024)(128)(2,1)}, u32[]{:S(2)}) copy-start(bf16[2048]{0:T(1024)(128)(2,1)} %param.33) | copy-start | bytes 12292
  115.4 21.3 %all-to-all-start.4 = ((bf16[16,16,2048]{2,1,0:T(8,128)(2,1)}), bf16[16,16,2048]{2,1,0:T(8,128)(2,1)S(1)}, u32[]{:S(2)}, u32[]{:S(2)}) async-start(bf16[16,16,2048]{2,1,0:T(8,128)(2,1)} %bitcast.129), calls=%async_computation.4 | async-start | bytes 2097152 | tf_op jit(solution)/shard_map/all_to_all | solution.py:177
where the time goes:
time: 139 us; the launch traced here: 138 us
  blocking collectives  43.9 us (32%)
  waiting for transfers between devices  28.1 us (20%)
  local copies, waits for them, and re-layouts  23 us (17%)
  starting transfers between devices  16 us (12%)
  other arithmetic  14.1 us (10%)
  matrix products  12.4 us (9%)
    all_to_all x1, blocking collectives, in_one_piece(): lax.all_to_all(both, axis, split_axis=split_dim, concat_axis=concat_dim,...  31.1 us
    all_gather x1, blocking collectives, per_device(): mixed_rows = lax.all_gather(mixed_part, 'tp', axis=1, tiled=True)  12.8 us
    all_to_all x1, waiting for transfers between devices, per_device(): lax.all_to_all(partial_rows.reshape(ep_count, per_dev, width).astype(jnp....  11.8 us
    all_to_all x1, waiting for transfers between devices, per_device(): lax.all_to_all(computed, 'ep', split_axis=0, concat_axis=0, tiled=True)  8.19 us
    reduce_sum x1, other arithmetic, per_device(): jnp.sum(jnp.where(is_mine, weights, 0.0)[..., None] * picked, axis=1)  6.28 us
    convert_element_type x1, local copies, waits for them, and re-layouts, per_device(): picked = flat_back[jnp.where(is_mine, slot_place, 0)].astype(jnp.float32)  4.75 us
    all_to_all x1, starting transfers between devices, from_everyone(): lax.all_to_all(jnp.broadcast_to(array[None], (length, *array.shape)), axi...  4.58 us
    all_to_all x1, starting transfers between devices, sent_and_summed(): lax.all_to_all(in_blocks(array, dim, length), axis, 0, 0, tiled=True)  4.14 us
  transfers between devices with their start and end apart: 4, of which 4 were waited for; matrix products, arithmetic and copies ran while one was open for 15% of the time, Pallas kernels for 0%

commit v1 on v0

--- a/solution.py
+++ b/solution.py
@@ -140,7 +140,7 @@
     mixed_part, new_state = mixer_step(
         normed, in_weight, state, decay_rate, frequency, log_step, in_coef, out_coef, skip_gain
     )
-    mixed_rows = lax.all_gather(mixed_part, "tp", axis=1, tiled=True)
+    mixed_rows = jnp.concatenate(lax.all_gather(mixed_part, "tp"), axis=1)
     after_mix = full_resid.astype(jnp.float32) + jnp.dot(
         mixed_rows, out_weight, preferred_element_type=jnp.float32
     )

time: 139 us -> 138 us (level)
  no operation moved by 1% of the time
where the time goes in v1:
time: 138 us; the launch traced here: 137 us
  blocking collectives  42.6 us (31%)
  waiting for transfers between devices  28.2 us (20%)
  local copies, waits for them, and re-layouts  23 us (17%)
  starting transfers between devices  16 us (12%)
  other arithmetic  14.1 us (10%)
  matrix products  12.4 us (9%)
    all_to_all x1, blocking collectives, in_one_piece(): lax.all_to_all(both, axis, split_axis=split_dim, concat_axis=concat_dim,...  31.1 us
    all_to_all x1, waiting for transfers between devices, per_device(): lax.all_to_all(partial_rows.reshape(ep_count, per_dev, width).astype(jnp....  11.8 us
    all_gather x1, blocking collectives, per_device(): mixed_rows = jnp.concatenate(lax.all_gather(mixed_part, 'tp'), axis=1)  11.5 us
    all_to_all x1, waiting for transfers between devices, per_device(): lax.all_to_all(computed, 'ep', split_axis=0, concat_axis=0, tiled=True)  8.2 us
    reduce_sum x1, other arithmetic, per_device(): jnp.sum(jnp.where(is_mine, weights, 0.0)[..., None] * picked, axis=1)  6.28 us
    convert_element_type x1, local copies, waits for them, and re-layouts, per_device(): picked = flat_back[jnp.where(is_mine, slot_place, 0)].astype(jnp.float32)  4.75 us
    all_to_all x1, starting transfers between devices, from_everyone(): lax.all_to_all(jnp.broadcast_to(array[None], (length, *array.shape)), axi...  4.58 us
    all_to_all x1, starting transfers between devices, sent_and_summed(): lax.all_to_all(in_blocks(array, dim, length), axis, 0, 0, tiled=True)  4.14 us
  transfers between devices with their start and end apart: 4, of which 4 were waited for; matrix products, arithmetic and copies ran while one was open for 15% of the time, Pallas kernels for 0%

profile of v1, /device:TPU:0, one launch (start us, length us, event | category | flops | bytes accessed | tf_op | source)
XLA Modules:
  0.0 137.2 jit_solution(3782610992156359546)
XLA Ops:
  0.7 1.8 %broadcast_in_dim.22 = bf16[8,128,256]{2,1,0:T(8,128)(2,1)} broadcast(bf16[128,256]{1,0:T(8,128)(2,1)} %param.21), dimensions={1,2} | broadcast | bytes 589824 | tf_op jit(solution)/shard_map/broadcast_in_dim | solution.py:19
  2.5 4.6 %all-to-all-start = ((bf16[8,128,256]{2,1,0:T(8,128)(2,1)}), bf16[8,128,256]{2,1,0:T(8,128)(2,1)S(1)}, u32[]{:S(2)}, u32[]{:S(2)}) async-start(bf16[8,128,256]{2,1,0:T(8,128)(2,1)} %broadcast_in_dim.22), calls=%async_computation | async-start | bytes 1048576 | tf_op jit(solution)/shard_map/all_to_all | solution.py:18
  7.1 0.8 copy.92
  7.8 0.1 eq.54
  8.0 0.1 eq.50
  8.1 0.7 exp.17
  8.7 0.7 reduce_sum.94
  9.4 0.7 multiply_select_fusion
  10.1 0.1 copy.98
  10.3 0.1 and.23
  10.4 0.1 copy.94
  10.6 0.1 broadcast_in_dim.25
  10.7 0.2 fusion.37
  11.0 0.2 fusion.26
  11.2 0.1 reshape.129
  11.4 0.1 copy.97
  11.5 0.1 eq.58
  11.6 1.1 fusion.78
  12.7 0.1 copy.88
  12.8 0.1 copy.89
  13.0 0.1 select_reduce_fusion
  13.2 0.1 add_divide_fusion
  13.3 4.1 %all-to-all-done = bf16[8,128,256]{2,1,0:T(8,128)(2,1)S(1)} async-done(((bf16[8,128,256]{2,1,0:T(8,128)(2,1)}), bf16[8,128,256]{2,1,0:T(8,128)(2,1)S(1)}, u32[]{:S(2)}, u32[]{:S(2)}) %all-to-all-start) | async-done | bytes 524320 | tf_op jit(solution)/shard_map/all_to_all | solution.py:18
  17.6 0.2 convert_reduce_fusion.1
  17.8 0.6 copy-done.7
  18.4 0.4 convolution_convert_fusion.2
  18.9 0.3 fusion.9
  19.2 0.3 fusion.10
  19.5 0.1 fusion.52
  19.6 0.1 convolution_subtract_fusion
  19.8 0.1 fusion.50
  19.9 11.5 %all-gather = bf16[1024,128]{0,1:T(8,128)(2,1)S(1)} all-gather(bf16[128,128]{0,1:T(8,128)(2,1)S(1)} %fusion.50), channel_id=2, replica_groups=mesh['ep'=16,'tp'=8] {'tp'}, dimensions={0}, use_global_device_ids=true | all-gather | bytes 294912 | tf_op jit(solution)/shard_map/all_gather | solution.py:143
  31.5 0.8 fusion.75
  32.4 1.0 copy-done.2
  33.3 0.2 multiply_convert_fusion
  33.6 0.9 gather_fusion
  34.5 0.1 broadcast_in_dim.32
  34.6 0.2 pad_maximum_fusion
  34.8 31.1 %all_to_all.25 = bf16[16,24,2048]{2,1,0:T(8,128)(2,1)S(1)} all-to-all(bf16[16,24,2048]{2,1,0:T(8,128)(2,1)S(1)} %pad_maximum_fusion), channel_id=1, replica_groups=mesh['ep'=16,'tp'=8] {'ep'}, dimensions={0} | all-to-all | bytes 3145728 | tf_op jit(solution)/shard_map/all_to_all | solution.py:30
  65.9 1.2 copy-done.1
  67.1 0.4 fusion.4
  67.5 3.4 %fusion = bf16[16,8,2048]{2,1,0:T(8,128)(2,1)} fusion(bf16[1,512,2048]{2,1,0:T(8,128)(2,1)S(1)} %copy-done, bf16[1,2048,512]{2,1,0:T(8,128)(2,1)} %param.37, bf16[16,24,2048]{2,1,0:T(8,128)(2,1)} %copy-done.1, f32[128,512]{1,0:T(8,128)S(1)} %fusion.4), kind=kOutput, calls=%fused_computation.6 | convolution fusion | flops 537526272 | bytes 5505024 | tf_op jit(solution)/shard_map/dot_general | solution.py:107
  70.9 3.6 %all-to-all-start.2 = ((bf16[16,8,2048]{2,1,0:T(8,128)(2,1)}), bf16[16,8,2048]{2,1,0:T(8,128)(2,1)S(1)}, u32[]{:S(2)}, u32[]{:S(2)}) async-start(bf16[16,8,2048]{2,1,0:T(8,128)(2,1)} %fusion), calls=%async_computation.2 | async-start | bytes 1048576 | tf_op jit(solution)/shard_map/all_to_all | solution.py:171
  74.5 0.1 copy.91
  74.6 0.1 copy.99
  74.7 0.1 reshape.146
  74.8 2.3 %slice.48 = bf16[16,16,2048]{2,1,0:T(8,128)(2,1)} slice(bf16[16,24,2048]{2,1,0:T(8,128)(2,1)} %copy-done.1), slice={[0:16], [8:24], [0:2048]} | slice | bytes 2097152 | tf_op jit(solution)/shard_map/slice | solution.py:35
  77.2 8.2 %all-to-all-done.2 = bf16[16,8,2048]{2,1,0:T(8,128)(2,1)S(1)} async-done(((bf16[16,8,2048]{2,1,0:T(8,128)(2,1)}), bf16[16,8,2048]{2,1,0:T(8,128)(2,1)S(1)}, u32[]{:S(2)}, u32[]{:S(2)}) %all-to-all-start.2) | async-done | bytes 524320 | tf_op jit(solution)/shard_map/all_to_all | solution.py:171
  85.4 3.3 %gather_fusion.1 = bf16[512,2048]{1,0:T(8,128)(2,1)} fusion(bf16[128,2048]{1,0:T(8,128)(2,1)S(1)} %bitcast.123, s32[1024]{0:T(1024)S(1)} %pad_clamp_fusion), kind=kCustom, calls=%fused_computation.1 | custom fusion | bytes 4196352 | tf_op jit(solution)/shard_map/gather | solution.py:187
  88.7 4.8 %reshape.155 = f32[128,4,2048]{2,1,0:T(4,128)} reshape(bf16[512,2048]{1,0:T(8,128)(2,1)} %gather_fusion.1) | data formatting | bytes 6291456 | tf_op jit(solution)/shard_map/convert_element_type | solution.py:187
  93.4 6.3 %multiply_reduce_fusion = bf16[128,2048]{1,0:T(8,128)(2,1)} fusion(f32[128,4,2048]{2,1,0:T(4,128)} %reshape.155, f32[128,4]{1,0:T(8,128)S(1)} %copy.91), kind=kLoop, calls=%fused_computation.2 | loop fusion | flops 1835008 | bytes 4720640 | tf_op jit(solution)/shard_map/reduce_sum | solution.py:188
  99.7 4.1 %all-to-all-start.3 = ((bf16[8,16,2048]{2,1,0:T(8,128)(2,1)}), bf16[8,16,2048]{2,1,0:T(8,128)(2,1)}, u32[]{:S(2)}, u32[]{:S(2)}) async-start(bf16[8,16,2048]{2,1,0:T(8,128)(2,1)} %bitcast.134), calls=%async_computation.3 | async-start | bytes 1048576 | tf_op jit(solution)/shard_map/all_to_all | solution.py:47
  103.9 2.4 %fusion.79 = f32[256,256]{1,0:T(8,128)} fusion(bf16[256,2048]{1,0:T(8,128)(2,1)S(1)} %bitcast.126, bf16[2048,256]{1,0:T(8,128)(2,1)} %param.39), kind=kOutput, calls=%fused_computation.130 | convolution fusion | flops 268435456 | bytes 2359296 | tf_op jit(solution)/shard_map/dot_general | solution.py:173
  106.2 3.9 %convolution_convert_fusion = bf16[256,2048]{1,0:T(8,128)(2,1)} fusion(bf16[256,2048]{1,0:T(8,128)(2,1)} %param.41, bf16[256,2048]{1,0:T(8,128)(2,1)S(1)} %bitcast.127, bf16[2048,256]{1,0:T(8,128)(2,1)} %param.40, f32[256,256]{1,0:T(8,128)} %fusion.79), kind=kOutput, calls=%fused_computation.3 | convolution fusion | flops 537788416 | bytes 4456448 | tf_op jit(solution)/shard_map/dot_general | solution.py:176
  110.2 4.0 %all-to-all-done.3 = bf16[8,16,2048]{2,1,0:T(8,128)(2,1)} async-done(((bf16[8,16,2048]{2,1,0:T(8,128)(2,1)}), bf16[8,16,2048]{2,1,0:T(8,128)(2,1)}, u32[]{:S(2)}, u32[]{:S(2)}) %all-to-all-start.3) | async-done | bytes 524320 | tf_op jit(solution)/shard_map/all_to_all | solution.py:47
  114.2 3.7 %all-to-all-start.4 = ((bf16[16,16,2048]{2,1,0:T(8,128)(2,1)}), bf16[16,16,2048]{2,1,0:T(8,128)(2,1)S(1)}, u32[]{:S(2)}, u32[]{:S(2)}) async-start(bf16[16,16,2048]{2,1,0:T(8,128)(2,1)} %bitcast.138), calls=%async_computation.4 | async-start | bytes 2097152 | tf_op jit(solution)/shard_map/all_to_all | solution.py:177
  117.9 1.8 %copy.101 = f32[1,128,512]{2,1,0:T(8,128)} copy(f32[1,128,512]{1,2,0:T(8,128)} %bitcast.133) | data formatting | bytes 524288 | tf_op jit(solution)/shard_map/stack;reshape | solution.py:90
  119.7 0.8 copy.100
  120.5 1.9 %pad_maximum_fusion.1 = f32[2,128,512]{2,1,0:T(8,128)} fusion(f32[1,128,512]{2,1,0:T(8,128)} %copy.101, f32[1,128,512]{2,1,0:T(8,128)} %copy.100), kind=kLoop, calls=%fused_computation.38 | loop fusion | flops 131072 | bytes 1048576 | tf_op jit(solution)/shard_map/stack | solution.py:90
  122.3 0.1 fusion.18
  122.5 1.1 convert_reduce_fusion.2
  123.6 11.8 %all-to-all-done.4 = bf16[16,16,2048]{2,1,0:T(8,128)(2,1)S(1)} async-done(((bf16[16,16,2048]{2,1,0:T(8,128)(2,1)}), bf16[16,16,2048]{2,1,0:T(8,128)(2,1)S(1)}, u32[]{:S(2)}, u32[]{:S(2)}) %all-to-all-start.4) | async-done | bytes 1048608 | tf_op jit(solution)/shard_map/all_to_all | solution.py:177
  135.5 0.1 convert_reduce_fusion
  135.6 1.6 %add_convert_fusion = bf16[16,2048]{1,0:T(8,128)(2,1)} fusion(f32[16,2048]{1,0:T(8,128)S(1)} %convert_reduce_fusion, f32[16,2048]{1,0:T(8,128)S(1)} %convert_reduce_fusion.2, f32[128,2048]{1,0:T(8,128)} %copy-done.2, s32[]{:T(128)S(6)} %select_n.41, f32[16]{0:T(128)S(1)} %fusion.18), kind=kLoop, calls=%fused_computation.63 | loop fusion | flops 131072 | bytes 458820 | tf_op jit(solution)/shard_map/convert_element_type | solution.py:191
  (50 shorter events, 0.6 us)
Async XLA Ops:
  0.6 66.9 %copy-start = (bf16[1,512,2048]{2,1,0:T(8,128)(2,1)S(1)}, bf16[1,512,2048]{2,1,0:T(8,128)(2,1)}, u32[]{:S(2)}) copy-start(bf16[1,512,2048]{2,1,0:T(8,128)(2,1)} %param.38) | copy-start | bytes 6291460
  0.6 10.7 %copy-start.10 = (s32[128,4]{0,1:T(4,128)S(1)}, s32[128,4]{0,1:T(4,128)}, u32[]{:S(2)}) copy-start(s32[128,4]{0,1:T(4,128)} %param.34) | copy-start | bytes 6148
  2.5 14.9 %all-to-all-start = ((bf16[8,128,256]{2,1,0:T(8,128)(2,1)}), bf16[8,128,256]{2,1,0:T(8,128)(2,1)S(1)}, u32[]{:S(2)}, u32[]{:S(2)}) async-start(bf16[8,128,256]{2,1,0:T(8,128)(2,1)} %broadcast_in_dim.22), calls=%async_computation | async-start | bytes 1048576 | tf_op jit(solution)/shard_map/all_to_all | solution.py:18
  10.5 2.6 %copy-start.13 = (f32[8,64]{1,0:T(8,128)S(1)}, f32[8,64]{1,0:T(8,128)}, u32[]{:S(2)}) copy-start(f32[8,64]{1,0:T(8,128)} %param.26) | copy-start | bytes 6148
  10.5 2.6 %copy-start.14 = (f32[8,64]{1,0:T(8,128)S(1)}, f32[8,64]{1,0:T(8,128)}, u32[]{:S(2)}) copy-start(f32[8,64]{1,0:T(8,128)} %param.25) | copy-start | bytes 6148
  13.3 4.6 %copy-start.11 = (f32[2048]{0:T(1024)S(1)}, f32[2048]{0:T(1024)}, u32[]{:S(2)}) copy-start(f32[2048]{0:T(1024)} %param.22) | copy-start | bytes 24580
  17.4 1.0 copy-start.7
  17.5 1.4 %copy-start.8 = (f32[2,8,64,16]{2,3,1,0:T(8,128)S(1)}, f32[2,8,64,16]{2,3,1,0:T(8,128)}, u32[]{:S(2)}) copy-start(f32[2,8,64,16]{2,3,1,0:T(8,128)} %param.28) | copy-start | bytes 196612
  17.6 1.9 %copy-start.9 = (f32[2,8,16,64]{3,2,1,0:T(8,128)S(1)}, f32[2,8,16,64]{3,2,1,0:T(8,128)}, u32[]{:S(2)}) copy-start(f32[2,8,16,64]{3,2,1,0:T(8,128)} %param.29) | copy-start | bytes 196612
  18.4 1.4 copy-start.16
  18.4 13.1 %copy-start.3 = (bf16[1024,2048]{1,0:T(8,128)(2,1)S(1)}, bf16[1024,2048]{1,0:T(8,128)(2,1)}, u32[]{:S(2)}) copy-start(bf16[1024,2048]{1,0:T(8,128)(2,1)} %param.31) | copy-start | bytes 12582916
  19.2 13.2 %copy-start.5 = (f32[128,8,64]{0,2,1:T(8,128)}, f32[128,8,64]{0,2,1:T(8,128)S(1)}, u32[]{:S(2)}) copy-start(f32[128,8,64]{0,2,1:T(8,128)S(1)} %fusion.9) | copy-start | bytes 786436
  31.5 1.9 %copy-start.12 = (f32[2048]{0:T(1024)S(1)}, f32[2048]{0:T(1024)}, u32[]{:S(2)}) copy-start(f32[2048]{0:T(1024)} %param.32) | copy-start | bytes 24580
  32.3 1.0 copy-start.2
  34.8 32.3 %copy-start.6 = (bf16[1,2048,512]{2,1,0:T(8,128)(2,1)S(1)}, bf16[1,2048,512]{2,1,0:T(8,128)(2,1)}, u32[]{:S(2)}) copy-start(bf16[1,2048,512]{2,1,0:T(8,128)(2,1)} %param.36) | copy-start | bytes 6291460
  65.9 1.2 copy-start.1
  70.9 14.4 %all-to-all-start.2 = ((bf16[16,8,2048]{2,1,0:T(8,128)(2,1)}), bf16[16,8,2048]{2,1,0:T(8,128)(2,1)S(1)}, u32[]{:S(2)}, u32[]{:S(2)}) async-start(bf16[16,8,2048]{2,1,0:T(8,128)(2,1)} %fusion), calls=%async_computation.2 | async-start | bytes 1048576 | tf_op jit(solution)/shard_map/all_to_all | solution.py:171
  93.4 10.4 %copy-start.4 = (bf16[16,16,2048]{2,1,0:T(8,128)(2,1)S(1)}, bf16[16,16,2048]{2,1,0:T(8,128)(2,1)}, u32[]{:S(2)}) copy-start(bf16[16,16,2048]{2,1,0:T(8,128)(2,1)} %slice.48) | copy-start | bytes 3145732
  99.7 14.5 %all-to-all-start.3 = ((bf16[8,16,2048]{2,1,0:T(8,128)(2,1)}), bf16[8,16,2048]{2,1,0:T(8,128)(2,1)}, u32[]{:S(2)}, u32[]{:S(2)}) async-start(bf16[8,16,2048]{2,1,0:T(8,128)(2,1)} %bitcast.134), calls=%async_computation.3 | async-start | bytes 1048576 | tf_op jit(solution)/shard_map/all_to_all | solution.py:47
  110.1 7.7 %copy-start.15 = (bf16[2048]{0:T(1024)(128)(2,1)S(1)}, bf16[2048]{0:T(1024)(128)(2,1)}, u32[]{:S(2)}) copy-start(bf16[2048]{0:T(1024)(128)(2,1)} %param.33) | copy-start | bytes 12292
  114.2 21.3 %all-to-all-start.4 = ((bf16[16,16,2048]{2,1,0:T(8,128)(2,1)}), bf16[16,16,2048]{2,1,0:T(8,128)(2,1)S(1)}, u32[]{:S(2)}, u32[]{:S(2)}) async-start(bf16[16,16,2048]{2,1,0:T(8,128)(2,1)} %bitcast.138), calls=%async_computation.4 | async-start | bytes 2097152 | tf_op jit(solution)/shard_map/all_to_all | solution.py:177
